TPU v7x, 32 devices: a whole 2x2x4 slice. The times are simulated.
32 devices in a mesh: grp: 2 (over y), ep: 4 (over z), tp: 4 (over x, core).
Axes of the slice: x: 2, y: 2, z: 4, core: 2. Of those that a mesh axis runs over, the one named last changes fastest.
Arguments:
- tokens: bfloat16 [2048, 2048], P(('grp', 'ep')), parts along dimension 0, may hold values from -6 to 6
- norm_gain: float32 [2048], replicated, may hold values from 0.1 to 1.9
- routing: int32 [2048, 2], P(('grp', 'ep')), parts along dimension 0, may hold values from 0 to 3, all different within a row; in each aligned block of 256 rows (0 to 255, 256 to 511, ...) at most 192 rows name the same one
- gate_weights: float32 [2048, 2], P(('grp', 'ep')), parts along dimension 0, may hold values from 0.2 to 2
- expert_gate: bfloat16 [4, 2048, 1024], P('ep', None, 'tp'), may hold values from -0.125 to 0.125
- expert_up: bfloat16 [4, 2048, 1024], P('ep', None, 'tp'), may hold values from -0.125 to 0.125
- expert_down: bfloat16 [4, 1024, 2048], P('ep', 'tp'), may hold values from -0.1875 to 0.1875
- shared_gate: bfloat16 [2048, 512], P(None, 'tp'), may hold values from -0.125 to 0.125
- shared_up: bfloat16 [2048, 512], P(None, 'tp'), may hold values from -0.125 to 0.125
- shared_down: bfloat16 [512, 2048], P('tp'), may hold values from -0.25 to 0.25
Outputs:
- mixed: bfloat16 [2048, 2048], P(('grp', 'ep'), 'tp'), parts along dimension 0
There are 2 independent parts, one for each index of `grp`. A program takes and returns all parts, laid end to end along the dimension named above; an argument that names none is the same for every part. Nothing has to cross between parts.
Inputs may be any that keep to these rules, and one draw needn't show every extreme that they name: `routing`: each row names 2 different experts. Within each aligned block of 256 rows no expert is named by more than 192 rows, and in every draw some block has an expert named by exactly 192 rows.
All inputs are finite; a program needn't handle non-finite values.
Results may differ from a plain program's by a relative error of at most 0.012.
Values may be sent and summed in bfloat16 or wider, within the bound.
A program may use at most 64 MiB of HBM per device.

v0:
```python
import jax
import jax.numpy as jnp
from jax import lax
from jax.experimental import pallas as pl
from jax.experimental.pallas import tpu as pltpu
from jax.sharding import PartitionSpec as P


def norm_rows(tokens, norm_gain):
    values = tokens.astype(jnp.float32)
    scale = lax.rsqrt(jnp.mean(values * values, axis=-1, keepdims=True) + 1e-06)
    return (values * scale * norm_gain).astype(jnp.bfloat16)


def body(
    tokens,
    norm_gain,
    routing,
    gate_weights,
    expert_gate,
    expert_up,
    expert_down,
    shared_gate,
    shared_up,
    shared_down,
):
    ep_count = lax.axis_size("ep")
    tp_count = lax.axis_size("tp")
    tok_rows, width = tokens.shape
    top = routing.shape[1]
    local_experts = expert_gate.shape[0]
    experts = ep_count * local_experts
    capacity = max(2, 3 * tok_rows * top // (2 * experts))
    quarter = width // tp_count
    arrived_rows = ep_count * capacity
    normed = norm_rows(tokens, norm_gain)
    flat_experts = routing.reshape(-1)
    assign = flat_experts.shape[0]
    onehot = (flat_experts[:, None] == jnp.arange(experts, dtype=jnp.int32)[None, :]).astype(
        jnp.float32
    )
    lower = (jnp.arange(assign)[:, None] >= jnp.arange(assign)[None, :]).astype(jnp.float32)
    running = jnp.dot(lower, onehot, precision=lax.Precision.HIGHEST)
    slot = (jnp.sum(running * onehot, axis=1) - 1.0).astype(jnp.int32)
    dest = flat_experts * capacity + slot
    owner = jnp.arange(assign, dtype=jnp.int32) // top
    slot_token = jnp.full((experts * capacity,), tok_rows, jnp.int32).at[dest].set(owner)
    padded = jnp.concatenate([normed, jnp.zeros((1, width), jnp.bfloat16)], axis=0)
    outgoing = padded[slot_token].reshape(experts, capacity, width)
    position = lax.axis_index("tp")
    own_columns = lax.dynamic_slice_in_dim(outgoing, position * quarter, quarter, 2)
    arrived = lax.all_to_all(own_columns, "ep", split_axis=0, concat_axis=0, tiled=True)
    piece = lax.all_gather(arrived, "tp", axis=2, tiled=True)
    count = piece.shape[2]
    piece = piece.reshape(ep_count, local_experts, capacity, count)
    local = 0
    rows = piece[:, local].reshape(arrived_rows, count)
    gate_rows = expert_gate[local]
    up_rows = expert_up[local]
    gate_list = [jnp.dot(rows, gate_rows, preferred_element_type=jnp.float32)]
    up_list = [jnp.dot(rows, up_rows, preferred_element_type=jnp.float32)]
    gate_all = jnp.stack(gate_list)
    up_all = jnp.stack(up_list)
    local = 0
    hidden = (jax.nn.silu(gate_all[local]) * up_all[local]).astype(jnp.bfloat16)
    term = jnp.dot(hidden, expert_down[local], preferred_element_type=jnp.float32)
    routed_list = [term.reshape(ep_count, capacity, width)]
    routed_terms = jnp.stack(routed_list, axis=1).reshape(experts * capacity, width)
    shared_gate_rows = jnp.dot(normed, shared_gate, preferred_element_type=jnp.float32)
    shared_up_rows = jnp.dot(normed, shared_up, preferred_element_type=jnp.float32)
    shared_hidden = (jax.nn.silu(shared_gate_rows) * shared_up_rows).astype(jnp.bfloat16)
    shared_term = jnp.dot(shared_hidden, shared_down, preferred_element_type=jnp.float32)
    routed_sum, shared_sum = (
        lax.psum_scatter(
            routed_terms.astype(jnp.bfloat16), "tp", scatter_dimension=1, tiled=True
        ).astype(jnp.float32),
        lax.psum_scatter(
            shared_term.astype(jnp.bfloat16), "tp", scatter_dimension=1, tiled=True
        ).astype(jnp.float32),
    )
    expert_out = routed_sum.astype(jnp.bfloat16).reshape(experts, capacity, quarter)
    returned = lax.all_to_all(expert_out, "ep", split_axis=0, concat_axis=0, tiled=True)
    picked = returned.reshape(experts * capacity, quarter)[dest]
    picked = picked.astype(jnp.float32).reshape(tok_rows, top, quarter)
    routed = jnp.sum(picked * gate_weights[:, :, None], axis=1)
    return (routed + shared_sum).astype(jnp.bfloat16)


MESH = pl.DeviceIdType.MESH


def silu(v):
    return v / (1.0 + jnp.exp(-v))


def dot32(a, b):
    return jnp.dot(a, b, preferred_element_type=jnp.float32)


def make_kernel(ep_count, capacity, halves):
    others = list(range(1, ep_count))
    part = capacity // halves
    items = list(range(len(others) * halves))

    def kernel(
        tok_ref, gain_ref, routing_ref, gw_ref, wg_hbm, wu_hbm, wd_hbm, sg_hbm, su_hbm, sd_hbm,
        out_ref,
        wg, wu, wd, sg, su, sd, nq, pt, zsend, xq, esend, erecv, keep, fsend, frecv, gsend, grecv,
        wsem, zs, zr, cs, cr, xs, xr, ds, dr, es, er, fs, fr, gs, gr,
    ):
        e = lax.axis_index("ep")
        t = lax.axis_index("tp")
        x = t // 2
        c = t % 2
        core = {"tp": t ^ 1}
        across = {"tp": t ^ 2}
        rows, width = tok_ref.shape
        quarter = width // 4

        def partner(i):
            return {"ep": e ^ (i // halves + 1)}

        barrier = pltpu.get_barrier_semaphore()
        for k in others:
            pl.semaphore_signal(barrier, inc=1, device_id={"ep": e ^ k}, device_id_type=MESH)
        pl.semaphore_signal(barrier, inc=1, device_id=core, device_id_type=MESH)
        pl.semaphore_signal(barrier, inc=1, device_id=across, device_id_type=MESH)

        loads = [
            pltpu.make_async_copy(a, b, wsem.at[i])
            for i, (a, b) in enumerate(
                [(wg_hbm, wg), (wu_hbm, wu), (sg_hbm, sg), (su_hbm, su), (wd_hbm, wd), (sd_hbm, sd)]
            )
        ]
        for load in loads:
            load.start()

        values = tok_ref[...].astype(jnp.float32)
        scale = lax.rsqrt(jnp.mean(values * values, axis=-1, keepdims=True) + 1e-06)
        normed = (values * scale * gain_ref[...]).astype(jnp.bfloat16)
        for q in range(4):
            nq[q] = normed[:, q * quarter:(q + 1) * quarter]

        named = lax.broadcasted_iota(jnp.int32, (16, rows), 0) ^ e
        hit = jnp.zeros((16, rows), jnp.float32)
        weight = jnp.zeros((16, rows), jnp.float32)
        for j in range(routing_ref.shape[0]):
            same = routing_ref[j:j + 1, :] == named
            hit = hit + jnp.where(same, 1.0, 0.0)
            weight = weight + jnp.where(same, gw_ref[j:j + 1, :], 0.0)
        weight = weight.T
        earlier = (
            lax.broadcasted_iota(jnp.int32, (rows, rows), 0)
            < lax.broadcasted_iota(jnp.int32, (rows, rows), 1)
        )
        earlier = jnp.where(earlier, 1.0, 0.0).astype(jnp.bfloat16)
        rank = dot32(hit.astype(jnp.bfloat16), earlier)
        rank = jnp.where(hit > 0.5, rank, -1.0)
        place = lax.broadcasted_iota(jnp.int32, (part, rows), 0)

        def remote(src, dst, send, recv, to):
            return pltpu.make_async_remote_copy(
                src_ref=src, dst_ref=dst, send_sem=send, recv_sem=recv,
                device_id=to, device_id_type=MESH,
            )

        zcopy, ccopy, xcopy, dcopy, ecopy, fcopy, gcopy = {}, {}, {}, {}, {}, {}, {}
        for i in items:
            k, h = i // halves + 1, i % halves
            wanted = (place + h * part).astype(jnp.float32)
            chosen = jnp.where(rank[k:k + 1, :] == wanted, 1.0, 0.0).astype(jnp.bfloat16)
            pt[i] = chosen
            zsend[i] = dot32(chosen, nq[t]).astype(jnp.bfloat16)
            if i == 0:
                pl.semaphore_wait(barrier, len(others) + 2)
            zcopy[i] = remote(zsend.at[i], xq.at[i, t], zs.at[i], zr.at[i], partner(i))
            zcopy[i].start()

        def columns(q):
            return pl.ds(pl.multiple_of(q * quarter, quarter), quarter)

        def hidden_of(pieces, w_gate, w_up):
            gate, up = 0.0, 0.0
            for q in range(4):
                gate = gate + dot32(pieces(q), w_gate[q * quarter:(q + 1) * quarter, :])
                up = up + dot32(pieces(q), w_up[q * quarter:(q + 1) * quarter, :])
            return (silu(gate) * up).astype(jnp.bfloat16)

        def exchange(r, n, product):
            for j in range(2):
                esend[r, j, :n] = product(columns(2 * j + 1 - c)).astype(jnp.bfloat16)
            ecopy[r] = remote(
                esend.at[r, :, pl.ds(0, n)], erecv.at[r, :, pl.ds(0, n)], es.at[r], er.at[r], core
            )
            ecopy[r].start()
            for j in range(2):
                keep[r, j, :n] = product(columns(2 * j + c))

        def arrive(i):
            zcopy[i].wait_recv()
            mine = xq.at[i, t]
            xcopy[i] = remote(mine, mine, xs.at[i], xr.at[i], across)
            xcopy[i].start()
            ccopy[i] = remote(mine, mine, cs.at[i], cr.at[i], core)
            ccopy[i].start()

        def relay(i):
            xcopy[i].wait_recv()
            theirs = xq.at[i, t ^ 2]
            dcopy[i] = remote(theirs, theirs, ds.at[i], dr.at[i], core)
            dcopy[i].start()

        def expert(i):
            ccopy[i].wait_recv()
            dcopy[i].wait_recv()
            hidden = hidden_of(lambda q: xq[i, q], wg, wu)
            exchange(1 + i, part, lambda cols: dot32(hidden, wd[:, cols]))

        def pair(r, n):
            ecopy[r].wait_recv()
            fsend[r, :n] = (
                keep[r, 1 - x, :n] + erecv[r, 1 - x, :n].astype(jnp.float32)
            ).astype(jnp.bfloat16)
            fcopy[r] = remote(
                fsend.at[r, pl.ds(0, n)], frecv.at[r, pl.ds(0, n)], fs.at[r], fr.at[r], across
            )
            fcopy[r].start()

        def whole(r, n):
            fcopy[r].wait_recv()
            return (
                keep[r, x, :n]
                + erecv[r, x, :n].astype(jnp.float32)
                + frecv[r, :n].astype(jnp.float32)
            )

        def give_back(i):
            gsend[i] = whole(1 + i, part).astype(jnp.bfloat16)
            gcopy[i] = remote(gsend.at[i], grecv.at[i], gs.at[i], gr.at[i], partner(i))
            gcopy[i].start()

        for load in loads:
            load.wait()
        own_hidden = hidden_of(lambda q: nq[q], wg, wu)
        shared_hidden = hidden_of(lambda q: nq[q], sg, su)
        exchange(
            0,
            rows,
            lambda cols: dot32(own_hidden, wd[:, cols]) * weight[:, 0:1]
            + dot32(shared_hidden, sd[:, cols]),
        )
        plan(arrive, relay, expert, pair, give_back, len(items), rows, part)

        total = whole(0, rows)
        for i in items:
            k = i // halves + 1
            gcopy[i].wait_recv()
            placed = lax.dot_general(
                pt[i], grecv[i], (((0,), (0,)), ((), ())), preferred_element_type=jnp.float32
            )
            total = total + placed * weight[:, k:k + 1]
        out_ref[...] = total.astype(out_ref.dtype)

        for group in (zcopy, ccopy, xcopy, dcopy, ecopy, fcopy, gcopy):
            for copy in group.values():
                copy.wait_send()

    return kernel


def plan(arrive, relay, expert, pair, give_back, count, rows, part):
    for step in range(count + 3):
        if step < count:
            arrive(step)
        if step == 0:
            pair(0, rows)
        if 0 <= step - 3 < count:
            give_back(step - 3)
        if 0 <= step - 1 < count:
            relay(step - 1)
        if 0 <= step - 2 < count:
            pair(1 + step - 2, part)
        if 0 <= step - 1 < count:
            expert(step - 1)


def fused_body(
    tokens, norm_gain, routing, gate_weights,
    expert_gate, expert_up, expert_down, shared_gate, shared_up, shared_down,
):
    n = lax.axis_size("ep")
    rows, width = tokens.shape
    capacity = max(2, 3 * rows * routing.shape[1] // (2 * n))
    quarter = width // 4
    ffe = expert_gate.shape[2]
    ffs = shared_gate.shape[1]
    halves = 2 if capacity % 32 == 0 else 1
    part = capacity // halves
    o = (n - 1) * halves
    bf16, f32 = jnp.bfloat16, jnp.float32
    big = max(rows, part)
    dma = pltpu.SemaphoreType.DMA
    vmem = pl.BlockSpec(memory_space=pltpu.VMEM)
    hbm = pl.BlockSpec(memory_space=pl.ANY)
    return pl.pallas_call(
        make_kernel(n, capacity, halves),
        out_shape=jax.ShapeDtypeStruct((rows, quarter), bf16),
        in_specs=[vmem] * 4 + [hbm] * 6,
        out_specs=vmem,
        scratch_shapes=[
            pltpu.VMEM((width, ffe), bf16),
            pltpu.VMEM((width, ffe), bf16),
            pltpu.VMEM((ffe, width), bf16),
            pltpu.VMEM((width, ffs), bf16),
            pltpu.VMEM((width, ffs), bf16),
            pltpu.VMEM((ffs, width), bf16),
            pltpu.VMEM((4, rows, quarter), bf16),
            pltpu.VMEM((o, part, rows), bf16),
            pltpu.VMEM((o, part, quarter), bf16),
            pltpu.VMEM((o, 4, part, quarter), bf16),
            pltpu.VMEM((o + 1, 2, big, quarter), bf16),
            pltpu.VMEM((o + 1, 2, big, quarter), bf16),
            pltpu.VMEM((o + 1, 2, big, quarter), f32),
            pltpu.VMEM((o + 1, big, quarter), bf16),
            pltpu.VMEM((o + 1, big, quarter), bf16),
            pltpu.VMEM((o, part, quarter), bf16),
            pltpu.VMEM((o, part, quarter), bf16),
            dma((6,)),
        ]
        + [dma((o,))] * 8
        + [dma((o + 1,))] * 4
        + [dma((o,))] * 2,
        compiler_params=pltpu.CompilerParams(collective_id=0, has_side_effects=True),
    )(
        tokens, norm_gain.reshape(1, width), routing.T, gate_weights.T,
        expert_gate[0], expert_up[0], expert_down[0], shared_gate, shared_up, shared_down,
    )


def solution(mesh):
    in_specs = (
        P(("grp", "ep"), None),
        P(),
        P(("grp", "ep"), None),
        P(("grp", "ep"), None),
        P("ep", None, "tp"),
        P("ep", None, "tp"),
        P("ep", "tp", None),
        P(None, "tp"),
        P(None, "tp"),
        P("tp", None),
    )
    out_specs = P(("grp", "ep"), "tp")
    ep_count, tp_count = mesh.shape["ep"], mesh.shape["tp"]

    def layer(*args):
        few = tp_count == 4 and ep_count in (2, 4) and args[4].shape[0] == ep_count
        chosen = fused_body if few else body
        return jax.shard_map(
            chosen, mesh=mesh, in_specs=in_specs, out_specs=out_specs, check_vma=False
        )(*args)

    return layer
```

profile of v0, /device:TPU:17, one launch (start us, length us, event | category | flops | bytes accessed | tf_op | source)
XLA Modules:
  0.0 56.7 jit_solution(15794173413324358805)
XLA Ops:
  0.0 55.0 %shard_map.100 = bf16[256,512]{1,0:T(8,128)(2,1)} custom-call(bf16[256,2048]{1,0:T(8,128)(2,1)} %tok_ref.1, f32[1,2048]{1,0:T(1,128)} %bitcast.9, s32[2,256]{1,0:T(2,128)} %bitcast.10, f32[2,256]{1,0:T(2,128)} %bitcast.11, bf16[2048,256]{1,0:T(8,128)(2,1)} %bitcast.6, bf16[2048,256]{1,0:T(8,128)(2,1)} %bitcast.7, bf16[256,2048]{1,0:T(8,128)(2,1)} %bitcast.8, ...), custom_call_target="tpu_custom_call" | custom-call | tf_op jit(solution)/shard_map/pallas_call | solution.py:305
  55.0 1.7 %copy.12 = bf16[256,512]{1,0:T(8,128)(2,1)} copy(bf16[256,512]{1,0:T(8,128)(2,1)} %shard_map.100) | data formatting | bytes 524288
where the time goes:
time: 56.8 us; the launch traced here: 56.7 us
  Pallas kernels  55 us (97%)
  local copies, waits for them, and re-layouts  1.67 us (3%)
    pallas_call x1, Pallas kernels, fused_body(): pl.pallas_call(make_kernel(n, capacity, halves), out_shape=jax.ShapeDtype...  55 us
    unnamed x1, local copies, waits for them, and re-layouts  1.67 us

commit v1 on v0

v1 whole, which is shorter than its diff:
```python
import jax
import jax.numpy as jnp
from jax import lax
from jax.experimental import pallas as pl
from jax.experimental.pallas import tpu as pltpu
from jax.sharding import PartitionSpec as P


def norm_rows(tokens, norm_gain):
    values = tokens.astype(jnp.float32)
    scale = lax.rsqrt(jnp.mean(values * values, axis=-1, keepdims=True) + 1e-06)
    return (values * scale * norm_gain).astype(jnp.bfloat16)


def body(
    tokens,
    norm_gain,
    routing,
    gate_weights,
    expert_gate,
    expert_up,
    expert_down,
    shared_gate,
    shared_up,
    shared_down,
):
    ep_count = lax.axis_size("ep")
    tp_count = lax.axis_size("tp")
    tok_rows, width = tokens.shape
    top = routing.shape[1]
    local_experts = expert_gate.shape[0]
    experts = ep_count * local_experts
    capacity = max(2, 3 * tok_rows * top // (2 * experts))
    quarter = width // tp_count
    arrived_rows = ep_count * capacity
    normed = norm_rows(tokens, norm_gain)
    flat_experts = routing.reshape(-1)
    assign = flat_experts.shape[0]
    onehot = (flat_experts[:, None] == jnp.arange(experts, dtype=jnp.int32)[None, :]).astype(
        jnp.float32
    )
    lower = (jnp.arange(assign)[:, None] >= jnp.arange(assign)[None, :]).astype(jnp.float32)
    running = jnp.dot(lower, onehot, precision=lax.Precision.HIGHEST)
    slot = (jnp.sum(running * onehot, axis=1) - 1.0).astype(jnp.int32)
    dest = flat_experts * capacity + slot
    owner = jnp.arange(assign, dtype=jnp.int32) // top
    slot_token = jnp.full((experts * capacity,), tok_rows, jnp.int32).at[dest].set(owner)
    padded = jnp.concatenate([normed, jnp.zeros((1, width), jnp.bfloat16)], axis=0)
    outgoing = padded[slot_token].reshape(experts, capacity, width)
    position = lax.axis_index("tp")
    own_columns = lax.dynamic_slice_in_dim(outgoing, position * quarter, quarter, 2)
    arrived = lax.all_to_all(own_columns, "ep", split_axis=0, concat_axis=0, tiled=True)
    piece = lax.all_gather(arrived, "tp", axis=2, tiled=True)
    count = piece.shape[2]
    piece = piece.reshape(ep_count, local_experts, capacity, count)
    local = 0
    rows = piece[:, local].reshape(arrived_rows, count)
    gate_rows = expert_gate[local]
    up_rows = expert_up[local]
    gate_list = [jnp.dot(rows, gate_rows, preferred_element_type=jnp.float32)]
    up_list = [jnp.dot(rows, up_rows, preferred_element_type=jnp.float32)]
    gate_all = jnp.stack(gate_list)
    up_all = jnp.stack(up_list)
    local = 0
    hidden = (jax.nn.silu(gate_all[local]) * up_all[local]).astype(jnp.bfloat16)
    term = jnp.dot(hidden, expert_down[local], preferred_element_type=jnp.float32)
    routed_list = [term.reshape(ep_count, capacity, width)]
    routed_terms = jnp.stack(routed_list, axis=1).reshape(experts * capacity, width)
    shared_gate_rows = jnp.dot(normed, shared_gate, preferred_element_type=jnp.float32)
    shared_up_rows = jnp.dot(normed, shared_up, preferred_element_type=jnp.float32)
    shared_hidden = (jax.nn.silu(shared_gate_rows) * shared_up_rows).astype(jnp.bfloat16)
    shared_term = jnp.dot(shared_hidden, shared_down, preferred_element_type=jnp.float32)
    routed_sum, shared_sum = (
        lax.psum_scatter(
            routed_terms.astype(jnp.bfloat16), "tp", scatter_dimension=1, tiled=True
        ).astype(jnp.float32),
        lax.psum_scatter(
            shared_term.astype(jnp.bfloat16), "tp", scatter_dimension=1, tiled=True
        ).astype(jnp.float32),
    )
    expert_out = routed_sum.astype(jnp.bfloat16).reshape(experts, capacity, quarter)
    returned = lax.all_to_all(expert_out, "ep", split_axis=0, concat_axis=0, tiled=True)
    picked = returned.reshape(experts * capacity, quarter)[dest]
    picked = picked.astype(jnp.float32).reshape(tok_rows, top, quarter)
    routed = jnp.sum(picked * gate_weights[:, :, None], axis=1)
    return (routed + shared_sum).astype(jnp.bfloat16)


MESH = pl.DeviceIdType.MESH


def silu(v):
    return v / (1.0 + jnp.exp(-v))


def dot32(a, b):
    return jnp.dot(a, b, preferred_element_type=jnp.float32)


OUTER = (
    "sp1", "own", "ap1", "pair", "s20", "s21", "s31", "wt", "ap0", "s30",
    "cp", "aF1", "sr0", "aF0", "gp0", "sp0", "aN0", "aN1", "cF", "gp1",
    "cN", "gF0", "gF1", "gN0", "gN1",
)
INNER = (
    "sp1", "s31", "s30", "own", "sp0", "aN1", "aN0", "ap1", "sr0", "wt",
    "aF0", "aF1", "cN", "s20", "s21", "cF", "pair", "gN0", "gN1", "ap0",
    "gF0", "gF1", "cp", "gp0", "gp1",
)
REDUNDANT = 1
LAST = (2, 3, 1)


def make_kernel(half, redundant):
    def kernel(
        tok_ref, gain_ref, routing_ref, gw_ref, wg_hbm, wu_hbm, wd_hbm, sg_hbm, su_hbm, sd_hbm,
        out_ref,
        wg, wu, wd, sg, su, sd, nq, pick, place, weight_ref,
        zsend, zred, xq, esend, erecv, own_keep, own_send, own_recv,
        fsend, frecv, keep, gsend, grecv,
        wsem, ws, wr, zs, zr, rs, rr, xs, xr, es, er, ps, pr, fs, fr, gs, gr,
    ):
        e = lax.axis_index("ep")
        t = lax.axis_index("tp")
        x = t // 2
        c = t % 2
        core = {"tp": t ^ 1}
        across = {"tp": t ^ 2}
        rows, width = tok_ref.shape
        quarter = width // 4

        barrier = pltpu.get_barrier_semaphore()
        for k in (1, 2, 3):
            for d in range(2):
                pl.semaphore_signal(
                    barrier, inc=1, device_id={"ep": e ^ k, "tp": 2 * x + d}, device_id_type=MESH
                )
        pl.semaphore_signal(barrier, inc=1, device_id=core, device_id_type=MESH)
        pl.semaphore_signal(barrier, inc=1, device_id=across, device_id_type=MESH)

        def meet():
            pl.semaphore_wait(barrier, 8)

        loads = [
            pltpu.make_async_copy(a, b, wsem.at[i])
            for i, (a, b) in enumerate(
                [
                    (wg_hbm, wg.at[c]), (wu_hbm, wu.at[c]), (wd_hbm, wd.at[c]),
                    (sg_hbm, sg), (su_hbm, su), (sd_hbm, sd),
                ]
            )
        ]
        for load in loads:
            load.start()

        values = tok_ref[...].astype(jnp.float32)
        scale = lax.rsqrt(jnp.mean(values * values, axis=-1, keepdims=True) + 1e-06)
        normed = (values * scale * gain_ref[...]).astype(jnp.bfloat16)
        for q in range(4):
            nq[q] = normed[:, q * quarter:(q + 1) * quarter]

        named = lax.broadcasted_iota(jnp.int32, (16, rows), 0) ^ e
        hit = jnp.zeros((16, rows), jnp.float32)
        weight = jnp.zeros((16, rows), jnp.float32)
        for j in range(routing_ref.shape[0]):
            same = routing_ref[j:j + 1, :] == named
            hit = hit + jnp.where(same, 1.0, 0.0)
            weight = weight + jnp.where(same, gw_ref[j:j + 1, :], 0.0)
        earlier = (
            lax.broadcasted_iota(jnp.int32, (rows, rows), 0)
            < lax.broadcasted_iota(jnp.int32, (rows, rows), 1)
        )
        earlier = jnp.where(earlier, 1.0, 0.0).astype(jnp.bfloat16)
        rank = dot32(hit.astype(jnp.bfloat16), earlier)
        rank = jnp.where(hit > 0.5, rank, -1.0)
        down = lax.broadcasted_iota(jnp.int32, (half, rows), 0).astype(jnp.float32)
        for k in (1, 2, 3):
            for d in range(2):
                pick[k - 1, d] = jnp.where(
                    rank[k:k + 1, :] == down + float(d * half), 1.0, 0.0
                ).astype(jnp.bfloat16)
        side = lax.broadcasted_iota(jnp.int32, (rows, half), 1).astype(jnp.float32)

        def finish_tables():
            weight_ref[...] = weight.T
            turned = rank.T
            for k in (1, 2, 3):
                for d in range(2):
                    place[k - 1, d] = jnp.where(
                        turned[:, k:k + 1] == side + float(d * half), 1.0, 0.0
                    ).astype(jnp.bfloat16)

        def remote(src, dst, send, recv, to):
            return pltpu.make_async_remote_copy(
                src_ref=src, dst_ref=dst, send_sem=send, recv_sem=recv,
                device_id=to, device_id_type=MESH,
            )

        def weight_copy(i):
            ref = (wg, wu, wd)[i].at[c]
            return remote(ref, ref, ws.at[i], wr.at[i], core)

        def zcopy(k, j):
            return remote(
                zsend.at[k - 1, j], xq.at[k - 1, 2 * x + j],
                zs.at[k - 1, j], zr.at[k - 1, j], {"ep": e ^ k},
            )

        def rcopy(j):
            return remote(
                zred.at[j], xq.at[0, 2 * (1 - x) + j], rs.at[j], rr.at[j], {"ep": e ^ 1}
            )

        def xcopy(k, j):
            mine = xq.at[k - 1, 2 * x + j]
            return remote(mine, mine, xs.at[k - 1, j], xr.at[k - 1, j], across)

        def ecopy():
            return remote(esend, erecv, es.at[0], er.at[0], core)

        def pcopy():
            return remote(own_send, own_recv, ps.at[0], pr.at[0], across)

        def fcopy(k, j):
            return remote(
                fsend.at[k - 1, j], frecv.at[k - 1, j],
                fs.at[k - 1, j], fr.at[k - 1, j], across,
            )

        def gcopy(k, j, d):
            return remote(
                gsend.at[k - 1, j], grecv.at[k - 1, d],
                gs.at[k - 1, j], gr.at[k - 1, d], {"ep": e ^ k, "tp": 2 * x + j},
            )

        def columns(q):
            return pl.ds(pl.multiple_of(q * quarter, quarter), quarter)

        def hidden_of(pieces, w_gate, w_up):
            gate, up = 0.0, 0.0
            for q in range(4):
                part = slice(q * quarter, (q + 1) * quarter)
                gate = gate + dot32(pieces(q), w_gate[part, :])
                up = up + dot32(pieces(q), w_up[part, :])
            return (silu(gate) * up).astype(jnp.bfloat16)

        def redundant_at(k, j):
            return k == 1 and j < redundant

        def run(order, far):
            first = [True]

            def begin(copy):
                if first[0]:
                    meet()
                    first[0] = False
                copy.start()

            seen = set()

            def ready(indices):
                for i in indices:
                    if i not in seen:
                        seen.add(i)
                        loads[i].wait()

            def tables():
                if "tables" not in seen:
                    seen.add("tables")
                    finish_tables()

            for step in order:
                if step == "own":
                    ready(range(6))
                    tables()
                    w_gate, w_up, w_down = wg.at[c], wu.at[c], wd.at[c]
                    own_hidden = hidden_of(lambda q: nq[q], w_gate, w_up)
                    shared_hidden = hidden_of(lambda q: nq[q], sg, su)

                    def product(cols):
                        return (
                            dot32(own_hidden, w_down[:, cols]) * weight_ref[:, 0:1]
                            + dot32(shared_hidden, sd[:, cols])
                        )

                    for j in range(2):
                        esend[j] = product(columns(2 * j + 1 - c)).astype(jnp.bfloat16)
                    begin(ecopy())
                    for j in range(2):
                        own_keep[j] = product(columns(2 * j + c))
                elif step == "pair":
                    ecopy().wait_recv()
                    own_send[...] = (
                        own_keep[1 - x] + erecv[1 - x].astype(jnp.float32)
                    ).astype(jnp.bfloat16)
                    pcopy().start()
                elif step == "wt":
                    for i in range(3):
                        ready([i])
                        begin(weight_copy(i))
                    tables()
                elif step[0] == "s":
                    j = int(step[2])
                    if step[1] == "r":
                        zred[j] = dot32(pick[0, c], nq[2 * (1 - x) + j]).astype(jnp.bfloat16)
                        begin(rcopy(j))
                    else:
                        k = 1 if step[1] == "p" else int(step[1])
                        zsend[k - 1, j] = dot32(pick[k - 1, c], nq[2 * x + j]).astype(jnp.bfloat16)
                        begin(zcopy(k, j))
                else:
                    k = 1 if step[1] == "p" else far[step[1]]
                    if step[0] == "a":
                        j = int(step[2])
                        zcopy(k, j).wait_recv()
                        if not redundant_at(k, j):
                            xcopy(k, j).start()
                    elif step[0] == "c":
                        if step == first_use(order):
                            for i in range(3):
                                weight_copy(i).wait_recv()
                        for j in range(2):
                            (rcopy(j) if redundant_at(k, j) else xcopy(k, j)).wait_recv()
                        hidden = [
                            hidden_of(lambda q: xq[k - 1, q], wg.at[d], wu.at[d]) for d in range(2)
                        ]

                        def result(cols):
                            return dot32(hidden[0], wd[0, :, cols]) + dot32(hidden[1], wd[1, :, cols])

                        for j in range(2):
                            fsend[k - 1, j] = result(columns(2 * (1 - x) + j)).astype(jnp.bfloat16)
                            fcopy(k, j).start()
                        for j in range(2):
                            keep[k - 1, j] = result(columns(2 * x + j))
                    else:
                        j = int(step[2])
                        fcopy(k, j).wait_recv()
                        gsend[k - 1, j] = (
                            keep[k - 1, j] + frecv[k - 1, j].astype(jnp.float32)
                        ).astype(jnp.bfloat16)
                        gcopy(k, j, c).start()

        inner = (e == 1) | (e == 2)

        @pl.when(inner)
        def _():
            run(INNER, {"N": 3, "F": 2})

        @pl.when(jnp.logical_not(inner))
        def _():
            run(OUTER, {"N": 2, "F": 3})

        pcopy().wait_recv()
        total = own_keep[x] + erecv[x].astype(jnp.float32) + own_recv[...].astype(jnp.float32)
        for k in LAST:
            back = 0.0
            for d in range(2):
                gcopy(k, 0, d).wait_recv()
                back = back + dot32(place[k - 1, d], grecv[k - 1, d])
            total = total + back * weight_ref[:, k:k + 1]
        out_ref[...] = total.astype(out_ref.dtype)

        for i in range(3):
            weight_copy(i).wait_send()
        ecopy().wait_send()
        pcopy().wait_send()
        for j in range(redundant):
            rcopy(j).wait_send()
        for k in (1, 2, 3):
            for j in range(2):
                zcopy(k, j).wait_send()
                if not redundant_at(k, j):
                    xcopy(k, j).wait_send()
                fcopy(k, j).wait_send()
                gcopy(k, j, c).wait_send()

    return kernel


def first_use(order):
    return [step for step in order if step[0] == "c"][0]


def fused_body(
    tokens, norm_gain, routing, gate_weights,
    expert_gate, expert_up, expert_down, shared_gate, shared_up, shared_down,
):
    rows, width = tokens.shape
    half = 3 * rows * routing.shape[1] // (2 * 4) // 2
    quarter = width // 4
    ffe = expert_gate.shape[2]
    ffs = shared_gate.shape[1]
    bf16, f32 = jnp.bfloat16, jnp.float32
    dma = pltpu.SemaphoreType.DMA
    vmem = pl.BlockSpec(memory_space=pltpu.VMEM)
    hbm = pl.BlockSpec(memory_space=pl.ANY)
    piece = (3, 2, half, quarter)
    return pl.pallas_call(
        make_kernel(half, REDUNDANT),
        out_shape=jax.ShapeDtypeStruct((rows, quarter), bf16),
        in_specs=[vmem] * 4 + [hbm] * 6,
        out_specs=vmem,
        scratch_shapes=[
            pltpu.VMEM((2, width, ffe), bf16),
            pltpu.VMEM((2, width, ffe), bf16),
            pltpu.VMEM((2, ffe, width), bf16),
            pltpu.VMEM((width, ffs), bf16),
            pltpu.VMEM((width, ffs), bf16),
            pltpu.VMEM((ffs, width), bf16),
            pltpu.VMEM((4, rows, quarter), bf16),
            pltpu.VMEM((3, 2, half, rows), bf16),
            pltpu.VMEM((3, 2, rows, half), bf16),
            pltpu.VMEM((rows, 16), f32),
            pltpu.VMEM(piece, bf16),
            pltpu.VMEM((2, half, quarter), bf16),
            pltpu.VMEM((3, 4, half, quarter), bf16),
            pltpu.VMEM((2, rows, quarter), bf16),
            pltpu.VMEM((2, rows, quarter), bf16),
            pltpu.VMEM((2, rows, quarter), f32),
            pltpu.VMEM((rows, quarter), bf16),
            pltpu.VMEM((rows, quarter), bf16),
            pltpu.VMEM(piece, bf16),
            pltpu.VMEM(piece, bf16),
            pltpu.VMEM(piece, f32),
            pltpu.VMEM(piece, bf16),
            pltpu.VMEM(piece, bf16),
            dma((6,)), dma((3,)), dma((3,)),
            dma((3, 2)), dma((3, 2)), dma((2,)), dma((2,)), dma((3, 2)), dma((3, 2)),
            dma((1,)), dma((1,)), dma((1,)), dma((1,)),
            dma((3, 2)), dma((3, 2)), dma((3, 2)), dma((3, 2)),
        ],
        compiler_params=pltpu.CompilerParams(collective_id=0, has_side_effects=True),
    )(
        tokens, norm_gain.reshape(1, width), routing.T, gate_weights.T,
        expert_gate[0], expert_up[0], expert_down[0], shared_gate, shared_up, shared_down,
    )


def solution(mesh):
    in_specs = (
        P(("grp", "ep"), None),
        P(),
        P(("grp", "ep"), None),
        P(("grp", "ep"), None),
        P("ep", None, "tp"),
        P("ep", None, "tp"),
        P("ep", "tp", None),
        P(None, "tp"),
        P(None, "tp"),
        P("tp", None),
    )
    out_specs = P(("grp", "ep"), "tp")
    ep_count, tp_count = mesh.shape["ep"], mesh.shape["tp"]

    def layer(*args):
        slots = 3 * args[0].shape[0] * args[2].shape[1] // (8 * mesh.shape["grp"] * ep_count)
        few = tp_count == 4 and ep_count == 4 and args[4].shape[0] == 4 and slots % 32 == 0
        chosen = fused_body if few else body
        return jax.shard_map(
            chosen, mesh=mesh, in_specs=in_specs, out_specs=out_specs, check_vma=False
        )(*args)

    return layer
```

time: 56.8 us -> 48.3 us (0.85)
  the two profiles are of different devices: /device:TPU:17 before, /device:TPU:0 now
where the time goes in v1:
time: 48.3 us; the launch traced here: 47.7 us
  Pallas kernels  46 us (95%)
  local copies, waits for them, and re-layouts  1.67 us (3%)
    pallas_call x1, Pallas kernels, fused_body(): pl.pallas_call(make_kernel(half, REDUNDANT), out_shape=jax.ShapeDtypeStru...  46 us
    unnamed x1, local copies, waits for them, and re-layouts  1.67 us

profile of v1, /device:TPU:0, one launch (start us, length us, event | category | flops | bytes accessed | tf_op | source)
XLA Modules:
  0.0 47.7 jit_solution(9266571149842018284)
XLA Ops:
  0.0 46.0 %shard_map.100 = bf16[256,512]{1,0:T(8,128)(2,1)} custom-call(bf16[256,2048]{1,0:T(8,128)(2,1)} %tok_ref.1, f32[1,2048]{1,0:T(1,128)} %bitcast.9, s32[2,256]{1,0:T(2,128)} %bitcast.10, f32[2,256]{1,0:T(2,128)} %bitcast.11, bf16[2048,256]{1,0:T(8,128)(2,1)} %bitcast.6, bf16[2048,256]{1,0:T(8,128)(2,1)} %bitcast.7, bf16[256,2048]{1,0:T(8,128)(2,1)} %bitcast.8, ...), custom_call_target="tpu_custom_call" | custom-call | tf_op jit(solution)/shard_map/pallas_call | solution.py:399
  46.0 1.7 %copy.12 = bf16[256,512]{1,0:T(8,128)(2,1)} copy(bf16[256,512]{1,0:T(8,128)(2,1)} %shard_map.100) | data formatting | bytes 524288

commit v2 on v1

--- a/solution.py
+++ b/solution.py
@@ -398,7 +398,7 @@
     piece = (3, 2, half, quarter)
     return pl.pallas_call(
         make_kernel(half, REDUNDANT),
-        out_shape=jax.ShapeDtypeStruct((rows, quarter), bf16),
+        out_shape=pltpu.VMEM((rows, quarter), bf16),
         in_specs=[vmem] * 4 + [hbm] * 6,
         out_specs=vmem,
         scratch_shapes=[

time: 48.3 us -> 46.6 us (0.965)
  local copies, waits for them, and re-layouts: 1.67 us -> 0.71 us
  Pallas kernels: 46 us -> 45.3 us
    unnamed x1, local copies, waits for them, and re-layouts: 1.67 us -> 0.71 us
    pallas_call x1, Pallas kernels: 46 us -> 45.3 us  [fused_body(): pl.pallas_call(make_kernel(half, REDUNDANT), out_shape=pltpu.VMEM((rows,...]
where the time goes in v2:
time: 46.6 us; the launch traced here: 46 us
  Pallas kernels  45.3 us (97%)
  local copies, waits for them, and re-layouts  0.71 us (2%)
    pallas_call x1, Pallas kernels, fused_body(): pl.pallas_call(make_kernel(half, REDUNDANT), out_shape=pltpu.VMEM((rows,...  45.3 us

profile of v2, /device:TPU:0, one launch (start us, length us, event | category | flops | bytes accessed | tf_op | source)
XLA Modules:
  0.0 46.0 jit_solution(8110455016497242909)
XLA Ops:
  0.0 45.3 %shard_map.100 = bf16[256,512]{1,0:T(8,128)(2,1)S(1)} custom-call(bf16[256,2048]{1,0:T(8,128)(2,1)} %tok_ref.1, f32[1,2048]{1,0:T(1,128)} %bitcast.9, s32[2,256]{1,0:T(2,128)} %bitcast.10, f32[2,256]{1,0:T(2,128)} %bitcast.11, bf16[2048,256]{1,0:T(8,128)(2,1)} %bitcast.6, bf16[2048,256]{1,0:T(8,128)(2,1)} %bitcast.7, bf16[256,2048]{1,0:T(8,128)(2,1)} %bitcast.8, ...), custom_call_target="tpu_custom_call" | custom-call | tf_op jit(solution)/shard_map/pallas_call | solution.py:399
  45.3 0.7 %copy.12 = bf16[256,512]{1,0:T(8,128)(2,1)} copy(bf16[256,512]{1,0:T(8,128)(2,1)S(1)} %shard_map.100) | data formatting | bytes 524288

commit v3 on v2

--- a/solution.py
+++ b/solution.py
@@ -98,27 +98,32 @@
 
 
 OUTER = (
-    "sp1", "own", "ap1", "pair", "s20", "s21", "s31", "wt", "ap0", "s30",
-    "cp", "aF1", "sr0", "aF0", "gp0", "sp0", "aN0", "aN1", "cF", "gp1",
-    "cN", "gF0", "gF1", "gN0", "gN1",
+    "s20", "sp3", "s30", "s32", "s22", "ap3", "s23", "s21", "wt", "sp2",
+    "ap2", "ap1", "sp0", "aF2", "s33", "s31", "sp1", "aF0", "ap0", "cp",
+    "sr0", "gp0", "gp1", "aF3", "sr1", "aF1", "own", "aN3", "aN2", "aN0",
+    "aN1", "cF", "cN", "pair", "gp3", "gp2", "gF1", "gF0", "gF3", "gN0",
+    "gF2", "gN2", "gN3", "gN1",
 )
 INNER = (
-    "sp1", "s31", "s30", "own", "sp0", "aN1", "aN0", "ap1", "sr0", "wt",
-    "aF0", "aF1", "cN", "s20", "s21", "cF", "pair", "gN0", "gN1", "ap0",
-    "gF0", "gF1", "cp", "gp0", "gp1",
+    "s33", "sp3", "wt", "far", "sr0", "sp2", "s30", "aN3", "sp1", "s32",
+    "ap3", "aF0", "s23", "s31", "sp0", "sr1", "aF1", "aN0", "s22", "aF2",
+    "aF3", "aN2", "ap2", "s20", "aN1", "cF", "ap1", "s21", "own", "cN",
+    "gF0", "gF2", "gF3", "gF1", "gN0", "ap0", "gN2", "cp", "gN3", "gN1",
+    "gp0", "pair", "gp3", "gp1", "gp2",
 )
-REDUNDANT = 1
+CHUNKS = 4
+REDUNDANT = 2
 LAST = (2, 3, 1)
 
 
-def make_kernel(half, redundant):
+def make_kernel(half, redundant, chunks):
     def kernel(
         tok_ref, gain_ref, routing_ref, gw_ref, wg_hbm, wu_hbm, wd_hbm, sg_hbm, su_hbm, sd_hbm,
         out_ref,
         wg, wu, wd, sg, su, sd, nq, pick, place, weight_ref,
         zsend, zred, xq, esend, erecv, own_keep, own_send, own_recv,
         fsend, frecv, keep, gsend, grecv,
-        wsem, ws, wr, zs, zr, rs, rr, xs, xr, es, er, ps, pr, fs, fr, gs, gr,
+        wsem, far_sem, ws, wr, zs, zr, rs, rr, xs, xr, es, er, ps, pr, fs, fr, gs, gr,
     ):
         e = lax.axis_index("ep")
         t = lax.axis_index("tp")
@@ -128,18 +133,30 @@
         across = {"tp": t ^ 2}
         rows, width = tok_ref.shape
         quarter = width // 4
+        part = chunks // 2
+        wide = quarter // part
+        inner = (e == 1) | (e == 2)
 
         barrier = pltpu.get_barrier_semaphore()
-        for k in (1, 2, 3):
+
+        def greet(k):
             for d in range(2):
                 pl.semaphore_signal(
                     barrier, inc=1, device_id={"ep": e ^ k, "tp": 2 * x + d}, device_id_type=MESH
                 )
+
+        greet(1)
         pl.semaphore_signal(barrier, inc=1, device_id=core, device_id_type=MESH)
         pl.semaphore_signal(barrier, inc=1, device_id=across, device_id_type=MESH)
 
-        def meet():
-            pl.semaphore_wait(barrier, 8)
+        @pl.when(inner)
+        def _():
+            greet(3)
+
+        def tell(i, k):
+            pl.semaphore_signal(
+                far_sem.at[i], inc=1, device_id={"ep": e ^ k}, device_id_type=MESH
+            )
 
         loads = [
             pltpu.make_async_copy(a, b, wsem.at[i])
@@ -155,9 +172,7 @@
 
         values = tok_ref[...].astype(jnp.float32)
         scale = lax.rsqrt(jnp.mean(values * values, axis=-1, keepdims=True) + 1e-06)
-        normed = (values * scale * gain_ref[...]).astype(jnp.bfloat16)
-        for q in range(4):
-            nq[q] = normed[:, q * quarter:(q + 1) * quarter]
+        nq[...] = (values * scale * gain_ref[...]).astype(jnp.bfloat16)
 
         named = lax.broadcasted_iota(jnp.int32, (16, rows), 0) ^ e
         hit = jnp.zeros((16, rows), jnp.float32)
@@ -202,17 +217,17 @@
 
         def zcopy(k, j):
             return remote(
-                zsend.at[k - 1, j], xq.at[k - 1, 2 * x + j],
+                zsend.at[k - 1, j], xq.at[k - 1, chunks * x + j],
                 zs.at[k - 1, j], zr.at[k - 1, j], {"ep": e ^ k},
             )
 
         def rcopy(j):
             return remote(
-                zred.at[j], xq.at[0, 2 * (1 - x) + j], rs.at[j], rr.at[j], {"ep": e ^ 1}
+                zred.at[j], xq.at[0, chunks * (1 - x) + j], rs.at[j], rr.at[j], {"ep": e ^ 1}
             )
 
         def xcopy(k, j):
-            mine = xq.at[k - 1, 2 * x + j]
+            mine = xq.at[k - 1, chunks * x + j]
             return remote(mine, mine, xs.at[k - 1, j], xr.at[k - 1, j], across)
 
         def ecopy():
@@ -229,34 +244,40 @@
 
         def gcopy(k, j, d):
             return remote(
-                gsend.at[k - 1, j], grecv.at[k - 1, d],
-                gs.at[k - 1, j], gr.at[k - 1, d], {"ep": e ^ k, "tp": 2 * x + j},
-            )
-
-        def columns(q):
-            return pl.ds(pl.multiple_of(q * quarter, quarter), quarter)
-
-        def hidden_of(pieces, w_gate, w_up):
-            gate, up = 0.0, 0.0
-            for q in range(4):
-                part = slice(q * quarter, (q + 1) * quarter)
-                gate = gate + dot32(pieces(q), w_gate[part, :])
-                up = up + dot32(pieces(q), w_up[part, :])
+                gsend.at[k - 1, j], grecv.at[k - 1, d, j % part],
+                gs.at[k - 1, j], gr.at[k - 1, d, j % part],
+                {"ep": e ^ k, "tp": 2 * x + j // part},
+            )
+
+        def columns(q, size):
+            return pl.ds(pl.multiple_of(q * size, size), size)
+
+        def hidden_of(values, w_gate, w_up):
+            gate = dot32(values, w_gate[...])
+            up = dot32(values, w_up[...])
             return (silu(gate) * up).astype(jnp.bfloat16)
 
         def redundant_at(k, j):
             return k == 1 and j < redundant
 
-        def run(order, far):
-            first = [True]
+        def run(order, far, middle):
+            seen = set()
 
             def begin(copy):
-                if first[0]:
-                    meet()
-                    first[0] = False
+                if "meet" not in seen:
+                    seen.add("meet")
+                    pl.semaphore_wait(barrier, 6 if middle else 4)
+                    if middle:
+                        tell(0, 1)
+                        tell(0, 3)
                 copy.start()
 
-            seen = set()
+            def know(k):
+                if ("far", k) not in seen and (k == 2 or (k == 3 and not middle)):
+                    seen.add(("far", k))
+                    pl.semaphore_wait(far_sem.at[k - 2], 1)
+                    if middle:
+                        tell(1, 1)
 
             def ready(indices):
                 for i in indices:
@@ -270,12 +291,14 @@
                     finish_tables()
 
             for step in order:
-                if step == "own":
+                if step == "far":
+                    know(2)
+                elif step == "own":
                     ready(range(6))
                     tables()
                     w_gate, w_up, w_down = wg.at[c], wu.at[c], wd.at[c]
-                    own_hidden = hidden_of(lambda q: nq[q], w_gate, w_up)
-                    shared_hidden = hidden_of(lambda q: nq[q], sg, su)
+                    own_hidden = hidden_of(nq[...], w_gate, w_up)
+                    shared_hidden = hidden_of(nq[...], sg, su)
 
                     def product(cols):
                         return (
@@ -284,10 +307,10 @@
                         )
 
                     for j in range(2):
-                        esend[j] = product(columns(2 * j + 1 - c)).astype(jnp.bfloat16)
+                        esend[j] = product(columns(2 * j + 1 - c, quarter)).astype(jnp.bfloat16)
                     begin(ecopy())
                     for j in range(2):
-                        own_keep[j] = product(columns(2 * j + c))
+                        own_keep[j] = product(columns(2 * j + c, quarter))
                 elif step == "pair":
                     ecopy().wait_recv()
                     own_send[...] = (
@@ -302,12 +325,23 @@
                 elif step[0] == "s":
                     j = int(step[2])
                     if step[1] == "r":
-                        zred[j] = dot32(pick[0, c], nq[2 * (1 - x) + j]).astype(jnp.bfloat16)
+                        zred[j] = dot32(
+                            pick[0, c], nq[:, columns(chunks * (1 - x) + j, wide)]
+                        ).astype(jnp.bfloat16)
                         begin(rcopy(j))
                     else:
                         k = 1 if step[1] == "p" else int(step[1])
-                        zsend[k - 1, j] = dot32(pick[k - 1, c], nq[2 * x + j]).astype(jnp.bfloat16)
-                        begin(zcopy(k, j))
+                        zsend[k - 1, j] = dot32(
+                            pick[k - 1, c], nq[:, columns(chunks * x + j, wide)]
+                        ).astype(jnp.bfloat16)
+                        if "meet" in seen:
+                            know(k)
+                            begin(zcopy(k, j))
+                        else:
+                            copy = zcopy(k, j)
+                            begin(NoCopy())
+                            know(k)
+                            copy.start()
                 else:
                     k = 1 if step[1] == "p" else far[step[1]]
                     if step[0] == "a":
@@ -319,20 +353,21 @@
                         if step == first_use(order):
                             for i in range(3):
                                 weight_copy(i).wait_recv()
-                        for j in range(2):
+                        for j in range(chunks):
                             (rcopy(j) if redundant_at(k, j) else xcopy(k, j)).wait_recv()
-                        hidden = [
-                            hidden_of(lambda q: xq[k - 1, q], wg.at[d], wu.at[d]) for d in range(2)
-                        ]
+                        rows_in = jnp.concatenate([xq[k - 1, q] for q in range(2 * chunks)], axis=1)
+                        hidden = [hidden_of(rows_in, wg.at[d], wu.at[d]) for d in range(2)]
 
                         def result(cols):
                             return dot32(hidden[0], wd[0, :, cols]) + dot32(hidden[1], wd[1, :, cols])
 
-                        for j in range(2):
-                            fsend[k - 1, j] = result(columns(2 * (1 - x) + j)).astype(jnp.bfloat16)
+                        for j in range(chunks):
+                            fsend[k - 1, j] = result(
+                                columns(chunks * (1 - x) + j, wide)
+                            ).astype(jnp.bfloat16)
                             fcopy(k, j).start()
-                        for j in range(2):
-                            keep[k - 1, j] = result(columns(2 * x + j))
+                        for j in range(chunks):
+                            keep[k - 1, j] = result(columns(chunks * x + j, wide))
                     else:
                         j = int(step[2])
                         fcopy(k, j).wait_recv()
@@ -341,23 +376,23 @@
                         ).astype(jnp.bfloat16)
                         gcopy(k, j, c).start()
 
-        inner = (e == 1) | (e == 2)
-
         @pl.when(inner)
         def _():
-            run(INNER, {"N": 3, "F": 2})
+            run(INNER, {"N": 3, "F": 2}, True)
 
         @pl.when(jnp.logical_not(inner))
         def _():
-            run(OUTER, {"N": 2, "F": 3})
+            run(OUTER, {"N": 2, "F": 3}, False)
 
         pcopy().wait_recv()
         total = own_keep[x] + erecv[x].astype(jnp.float32) + own_recv[...].astype(jnp.float32)
         for k in LAST:
             back = 0.0
             for d in range(2):
-                gcopy(k, 0, d).wait_recv()
-                back = back + dot32(place[k - 1, d], grecv[k - 1, d])
+                for j in range(part):
+                    gcopy(k, j, d).wait_recv()
+                returned = jnp.concatenate([grecv[k - 1, d, j] for j in range(part)], axis=1)
+                back = back + dot32(place[k - 1, d], returned)
             total = total + back * weight_ref[:, k:k + 1]
         out_ref[...] = total.astype(out_ref.dtype)
 
@@ -368,7 +403,7 @@
         for j in range(redundant):
             rcopy(j).wait_send()
         for k in (1, 2, 3):
-            for j in range(2):
+            for j in range(chunks):
                 zcopy(k, j).wait_send()
                 if not redundant_at(k, j):
                     xcopy(k, j).wait_send()
@@ -376,6 +411,11 @@
                 gcopy(k, j, c).wait_send()
 
     return kernel
+
+
+class NoCopy:
+    def start(self):
+        pass
 
 
 def first_use(order):
@@ -395,9 +435,11 @@
     dma = pltpu.SemaphoreType.DMA
     vmem = pl.BlockSpec(memory_space=pltpu.VMEM)
     hbm = pl.BlockSpec(memory_space=pl.ANY)
-    piece = (3, 2, half, quarter)
+    chunks = CHUNKS
+    wide = 2 * quarter // chunks
+    piece = (3, chunks, half, wide)
     return pl.pallas_call(
-        make_kernel(half, REDUNDANT),
+        make_kernel(half, REDUNDANT, chunks),
         out_shape=pltpu.VMEM((rows, quarter), bf16),
         in_specs=[vmem] * 4 + [hbm] * 6,
         out_specs=vmem,
@@ -408,13 +450,13 @@
             pltpu.VMEM((width, ffs), bf16),
             pltpu.VMEM((width, ffs), bf16),
             pltpu.VMEM((ffs, width), bf16),
-            pltpu.VMEM((4, rows, quarter), bf16),
+            pltpu.VMEM((rows, width), bf16),
             pltpu.VMEM((3, 2, half, rows), bf16),
             pltpu.VMEM((3, 2, rows, half), bf16),
             pltpu.VMEM((rows, 16), f32),
             pltpu.VMEM(piece, bf16),
-            pltpu.VMEM((2, half, quarter), bf16),
-            pltpu.VMEM((3, 4, half, quarter), bf16),
+            pltpu.VMEM((max(REDUNDANT, 1), half, wide), bf16),
+            pltpu.VMEM((3, 2 * chunks, half, wide), bf16),
             pltpu.VMEM((2, rows, quarter), bf16),
             pltpu.VMEM((2, rows, quarter), bf16),
             pltpu.VMEM((2, rows, quarter), f32),
@@ -424,11 +466,12 @@
             pltpu.VMEM(piece, bf16),
             pltpu.VMEM(piece, f32),
             pltpu.VMEM(piece, bf16),
-            pltpu.VMEM(piece, bf16),
-            dma((6,)), dma((3,)), dma((3,)),
-            dma((3, 2)), dma((3, 2)), dma((2,)), dma((2,)), dma((3, 2)), dma((3, 2)),
+            pltpu.VMEM((3, 2, chunks // 2, half, wide), bf16),
+            dma((6,)), pltpu.SemaphoreType.REGULAR((2,)), dma((3,)), dma((3,)),
+            dma((3, chunks)), dma((3, chunks)), dma((chunks,)), dma((chunks,)),
+            dma((3, chunks)), dma((3, chunks)),
             dma((1,)), dma((1,)), dma((1,)), dma((1,)),
-            dma((3, 2)), dma((3, 2)), dma((3, 2)), dma((3, 2)),
+            dma((3, chunks)), dma((3, chunks)), dma((3, chunks)), dma((3, 2, chunks // 2)),
         ],
         compiler_params=pltpu.CompilerParams(collective_id=0, has_side_effects=True),
     )(

time: 46.6 us -> 46.2 us (level)
  no operation moved by 1% of the time
where the time goes in v3:
time: 46.2 us; the launch traced here: 46.1 us
  Pallas kernels  45.4 us (98%)
  local copies, waits for them, and re-layouts  0.71 us (2%)
    pallas_call x1, Pallas kernels, fused_body(): pl.pallas_call(make_kernel(half, REDUNDANT, chunks), out_shape=pltpu.VMEM...  45.4 us

profile of v3, /device:TPU:0, one launch (start us, length us, event | category | flops | bytes accessed | tf_op | source)
XLA Modules:
  0.0 46.1 jit_solution(12631969938462486651)
XLA Ops:
  0.0 45.4 %shard_map.100 = bf16[256,512]{1,0:T(8,128)(2,1)S(1)} custom-call(bf16[256,2048]{1,0:T(8,128)(2,1)} %tok_ref.1, f32[1,2048]{1,0:T(1,128)} %bitcast.9, s32[2,256]{1,0:T(2,128)} %bitcast.10, f32[2,256]{1,0:T(2,128)} %bitcast.11, bf16[2048,256]{1,0:T(8,128)(2,1)} %bitcast.6, bf16[2048,256]{1,0:T(8,128)(2,1)} %bitcast.7, bf16[256,2048]{1,0:T(8,128)(2,1)} %bitcast.8, ...), custom_call_target="tpu_custom_call" | custom-call | tf_op jit(solution)/shard_map/pallas_call | solution.py:441
  45.4 0.7 %copy.12 = bf16[256,512]{1,0:T(8,128)(2,1)} copy(bf16[256,512]{1,0:T(8,128)(2,1)S(1)} %shard_map.100) | data formatting | bytes 524288

commit v4 on v3

--- a/solution.py
+++ b/solution.py
@@ -98,21 +98,17 @@
 
 
 OUTER = (
-    "s20", "sp3", "s30", "s32", "s22", "ap3", "s23", "s21", "wt", "sp2",
-    "ap2", "ap1", "sp0", "aF2", "s33", "s31", "sp1", "aF0", "ap0", "cp",
-    "sr0", "gp0", "gp1", "aF3", "sr1", "aF1", "own", "aN3", "aN2", "aN0",
-    "aN1", "cF", "cN", "pair", "gp3", "gp2", "gF1", "gF0", "gF3", "gN0",
-    "gF2", "gN2", "gN3", "gN1",
+    "own", "s21", "s20", "sp1", "pair", "sr0", "s31", "aN0", "aN1", "s30",
+    "ap1", "ap0", "wt", "aF1", "sp0", "aF0", "cN", "cF", "gN0", "cp",
+    "gN1", "gF0", "gF1", "gp0", "gp1",
 )
 INNER = (
-    "s33", "sp3", "wt", "far", "sr0", "sp2", "s30", "aN3", "sp1", "s32",
-    "ap3", "aF0", "s23", "s31", "sp0", "sr1", "aF1", "aN0", "s22", "aF2",
-    "aF3", "aN2", "ap2", "s20", "aN1", "cF", "ap1", "s21", "own", "cN",
-    "gF0", "gF2", "gF3", "gF1", "gN0", "ap0", "gN2", "cp", "gN3", "gN1",
-    "gp0", "pair", "gp3", "gp1", "gp2",
+    "sp1", "far", "wt", "s20", "own", "sp0", "s21", "aF1", "sr0", "s31",
+    "aF0", "ap1", "s30", "cF", "aN1", "ap0", "gF0", "gF1", "aN0", "cp",
+    "cN", "gp0", "gN0", "pair", "gp1", "gN1",
 )
-CHUNKS = 4
-REDUNDANT = 2
+CHUNKS = 2
+REDUNDANT = 1
 LAST = (2, 3, 1)
 
 
@@ -353,13 +349,25 @@
                         if step == first_use(order):
                             for i in range(3):
                                 weight_copy(i).wait_recv()
-                        for j in range(chunks):
-                            (rcopy(j) if redundant_at(k, j) else xcopy(k, j)).wait_recv()
-                        rows_in = jnp.concatenate([xq[k - 1, q] for q in range(2 * chunks)], axis=1)
-                        hidden = [hidden_of(rows_in, wg.at[d], wu.at[d]) for d in range(2)]
+                        gates, ups = [0.0, 0.0], [0.0, 0.0]
+                        for side_x in (x, 1 - x):
+                            if side_x is not x:
+                                for j in range(chunks):
+                                    (rcopy(j) if redundant_at(k, j) else xcopy(k, j)).wait_recv()
+                            part_in = jnp.concatenate(
+                                [xq[k - 1, chunks * side_x + q] for q in range(chunks)], axis=1
+                            )
+                            deep = columns(side_x, width // 2)
+                            for d in range(2):
+                                gates[d] = gates[d] + dot32(part_in, wg[d, deep, :])
+                                ups[d] = ups[d] + dot32(part_in, wu[d, deep, :])
+                        hidden = jnp.concatenate(
+                            [(silu(gates[d]) * ups[d]).astype(jnp.bfloat16) for d in range(2)], axis=1
+                        )
 
                         def result(cols):
-                            return dot32(hidden[0], wd[0, :, cols]) + dot32(hidden[1], wd[1, :, cols])
+                            both = jnp.concatenate([wd[0, :, cols], wd[1, :, cols]], axis=0)
+                            return dot32(hidden, both)
 
                         for j in range(chunks):
                             fsend[k - 1, j] = result(

time: 46.2 us -> 46 us (level); the launches traced: 46.1 us -> 45.3 us
  Pallas kernels: 45.4 us -> 44.6 us
    pallas_call x1, Pallas kernels: 45.4 us -> 44.6 us  [fused_body(): pl.pallas_call(make_kernel(half, REDUNDANT, chunks), out_shape=pltpu.VMEM...]
where the time goes in v4:
time: 46 us; the launch traced here: 45.3 us
  Pallas kernels  44.6 us (97%)
  local copies, waits for them, and re-layouts  0.71 us (2%)
    pallas_call x1, Pallas kernels, fused_body(): pl.pallas_call(make_kernel(half, REDUNDANT, chunks), out_shape=pltpu.VMEM...  44.6 us

profile of v4, /device:TPU:0, one launch (start us, length us, event | category | flops | bytes accessed | tf_op | source)
XLA Modules:
  0.0 45.3 jit_solution(7780049797863992095)
XLA Ops:
  0.0 44.6 %shard_map.100 = bf16[256,512]{1,0:T(8,128)(2,1)S(1)} custom-call(bf16[256,2048]{1,0:T(8,128)(2,1)} %tok_ref.1, f32[1,2048]{1,0:T(1,128)} %bitcast.9, s32[2,256]{1,0:T(2,128)} %bitcast.10, f32[2,256]{1,0:T(2,128)} %bitcast.11, bf16[2048,256]{1,0:T(8,128)(2,1)} %bitcast.6, bf16[2048,256]{1,0:T(8,128)(2,1)} %bitcast.7, bf16[256,2048]{1,0:T(8,128)(2,1)} %bitcast.8, ...), custom_call_target="tpu_custom_call" | custom-call | tf_op jit(solution)/shard_map/pallas_call | solution.py:449
  44.6 0.7 %copy.12 = bf16[256,512]{1,0:T(8,128)(2,1)} copy(bf16[256,512]{1,0:T(8,128)(2,1)S(1)} %shard_map.100) | data formatting | bytes 524288
